TPU v7x, 512 devices: a whole 4x8x8 slice. The times are simulated.
512 devices in a mesh: fs: 64 (over z, y), tp: 8 (over x, core).
Axes of the slice: x: 4, y: 8, z: 8, core: 2. Of those that a mesh axis runs over, the one named last changes fastest.
Arguments:
- tokens: bfloat16 [24576, 2048], P('fs', 'tp'), may hold values from -24 to 24, as said below
- mixer_gain: float32 [2048], replicated, may hold values from 0.1 to 1.9
- w_content: float32 [2048, 1024], P('fs', 'tp'), may hold values from -0.125 to 0.125
- w_spatial: float32 [2048, 1024], P('fs', 'tp'), may hold values from -0.125 to 0.125
- content_scale: float32 [1024], P('tp'), may hold values from 0.5 to 2
- spatial_scale: float32 [1024], P('tp'), may hold values from 0.2 to 3.5, as said below
- spatial_gain: float32 [1024], P('tp'), may hold values from 0.1 to 1.9
- block_mixing: bfloat16 [8, 128, 128], P('tp'), may hold values from -0.5 to 0.5
- block_bias: float32 [8, 128], P('tp'), may hold values from -6 to 6
- w_project: float32 [1024, 2048], P('tp', 'fs'), may hold values from -0.1875 to 0.1875
- project_scale: float32 [2048], P('fs'), may hold values from 0.5 to 2
- channel_gain: float32 [2048], replicated, may hold values from 0.1 to 1.9
- w_up: float32 [2048, 8192], P('fs', 'tp'), may hold values from -0.125 to 0.125
- up_scale: float32 [8192], P('tp'), may hold values from 0.5 to 2
- w_down: float32 [8192, 2048], P('tp', 'fs'), may hold values from -0.0625 to 0.0625
- down_scale: float32 [2048], P('fs'), may hold values from 0.5 to 2
Outputs:
- layer_out: bfloat16 [24576, 2048], P('fs', 'tp')
Inputs may be any that keep to these rules, and one draw needn't show every extreme that they name: `tokens`: activations whose features and rows have differing scales. `spatial_scale`: positive column scales.
All inputs are finite; a program needn't handle non-finite values.
Results may differ from a plain program's by a relative error of at most 0.019.
Values may be sent and summed in bfloat16 or wider, within the bound.
A program may use at most 64 MiB of HBM per device.

v0:
```python
import jax
import jax.numpy as jnp
from jax import lax
from jax.sharding import PartitionSpec as P

EPSILON = 1e-06


def gather_turned(arrays, axis, dims):
    turned = [jnp.moveaxis(a, dim, 0) for a, dim in zip(arrays, dims)]
    both = jnp.concatenate([t.reshape(len(t), -1) for t in turned], axis=1)
    result, at, finished = (lax.all_gather(both, axis, axis=0, tiled=True), 0, [])
    for t, dim in zip(turned, dims):
        section = result[:, at : at + t[0].size].reshape(-1, *t.shape[1:])
        finished.append(jnp.moveaxis(section, 0, dim))
        at += t[0].size
    return tuple(finished)


def in_order(blocks, dim):
    blocks = jnp.moveaxis(blocks, 0, dim)
    dims = blocks.shape
    return blocks.reshape(*dims[:dim], dims[dim] * dims[dim + 1], *dims[dim + 2 :])


def sent_to_all(shard, axis):
    size = lax.axis_size(axis)
    return lax.all_to_all(
        jnp.broadcast_to(shard[None], (size, *shard.shape)), axis, 0, 0, tiled=True
    )


def gathered_copies(shard, axis, dim):
    return in_order(sent_to_all(shard, axis), dim)


def over_copies(shard, axis):
    return sent_to_all(shard, axis).sum(axis=0)


def in_blocks(shard, dim, size):
    before, after = (shard.shape[:dim], shard.shape[dim + 1 :])
    return jnp.moveaxis(shard.reshape(*before, size, -1, *after), dim, 0)


def summed_on_arrival(shard, axis, dim):
    size = lax.axis_size(axis)
    blocks = lax.all_to_all(in_blocks(shard, dim, size), axis, 0, 0, tiled=True)
    return jnp.sum(blocks.astype(jnp.float32), axis=0)


def normalize_rows(token_rows, gain_vector):
    values = token_rows.astype(jnp.float32)
    scaled = values * lax.rsqrt(jnp.mean(values * values, axis=-1, keepdims=True) + EPSILON)
    return (scaled * gain_vector).astype(jnp.bfloat16)


def shards(
    tokens,
    mixer_gain,
    w_content,
    w_spatial,
    content_scale,
    spatial_scale,
    spatial_gain,
    block_mixing,
    block_bias,
    w_project,
    project_scale,
    channel_gain,
    w_up,
    up_scale,
    w_down,
    down_scale,
):
    content_weight = w_content.astype(jnp.bfloat16)
    spatial_weight = w_spatial.astype(jnp.bfloat16)
    project_weight = w_project.astype(jnp.bfloat16)
    up_weight = w_up.astype(jnp.bfloat16)
    down_weight = w_down.astype(jnp.bfloat16)
    project_full, down_full = gather_turned((project_scale, down_scale), "fs", (0, 0))
    gathered_rows = gathered_copies(tokens, "tp", 1)
    normed = normalize_rows(gathered_rows, mixer_gain)
    row_count = gathered_rows.shape[0]
    content_full, spatial_full, project_cols = gather_turned(
        (content_weight, spatial_weight, project_weight), "fs", (0, 0, 1)
    )
    content_linear = jnp.dot(normed, content_full, preferred_element_type=jnp.float32)
    spatial_linear = jnp.dot(normed, spatial_full, preferred_element_type=jnp.float32)
    content = jax.nn.gelu(content_linear * content_scale)
    spatial = jax.nn.gelu(spatial_linear * spatial_scale)
    square_sums = over_copies(jnp.sum(spatial * spatial, axis=1), "tp")
    total_width = spatial.shape[1] * lax.axis_size("tp")
    spatial_norm = (
        spatial * lax.rsqrt(square_sums / total_width + EPSILON)[:, None] * spatial_gain
    ).astype(jnp.bfloat16)
    groups_here = block_mixing.shape[0]
    block_size = block_mixing.shape[1]
    group_width = spatial_norm.shape[1] // groups_here
    causal_mask = jnp.tril(jnp.ones((block_size, block_size), dtype=bool))
    mixing_weights = jnp.where(causal_mask[None, :, :], block_mixing, jnp.zeros_like(block_mixing))
    grouped = spatial_norm.reshape(row_count // block_size, block_size, groups_here, group_width)
    mixed_block = (
        jnp.einsum("gts,nsgc->ntgc", mixing_weights, grouped, preferred_element_type=jnp.float32)
        + block_bias.T[None, :, :, None]
    )
    gated = (content * mixed_block.reshape(row_count, spatial_norm.shape[1])).astype(jnp.bfloat16)
    mixer_terms = jnp.dot(gated, project_cols, preferred_element_type=jnp.float32) * project_full
    mixer_sum = summed_on_arrival(mixer_terms.astype(jnp.bfloat16), "tp", 1)
    middle = (tokens.astype(jnp.float32) + mixer_sum).astype(jnp.bfloat16)
    middle_rows = gathered_copies(middle, "tp", 1)
    channel_normed = normalize_rows(middle_rows, channel_gain)
    up_full, down_cols = gather_turned((up_weight, down_weight), "fs", (0, 1))
    up_linear = jnp.dot(channel_normed, up_full, preferred_element_type=jnp.float32)
    hidden = jnp.square(jax.nn.relu(up_linear * up_scale)).astype(jnp.bfloat16)
    channel_terms = jnp.dot(hidden, down_cols, preferred_element_type=jnp.float32) * down_full
    channel_sum = summed_on_arrival(channel_terms.astype(jnp.bfloat16), "tp", 1)
    return (middle.astype(jnp.float32) + channel_sum).astype(jnp.bfloat16)


def solution(mesh):
    return jax.shard_map(
        shards,
        mesh=mesh,
        in_specs=(
            P("fs", "tp"),
            P(),
            P("fs", "tp"),
            P("fs", "tp"),
            P("tp"),
            P("tp"),
            P("tp"),
            P("tp", None, None),
            P("tp", None),
            P("tp", "fs"),
            P("fs"),
            P(),
            P("fs", "tp"),
            P("tp"),
            P("tp", "fs"),
            P("fs"),
        ),
        out_specs=P("fs", "tp"),
        check_vma=False,
    )
```

profile of v0, /device:TPU:1, one launch (start us, length us, event | category | flops | bytes accessed | tf_op | source)
XLA Modules:
  0.0 238.0 jit_solution(6624533297289008726)
XLA Ops:
  6.5 0.7 convert_bitcast_fusion.1
  7.3 0.7 convert_element_type.86
  8.0 0.7 convert_element_type.87
  8.7 0.6 pad_maximum_fusion.1
  9.3 0.0 all-gather.4.cloned.1.call-update
  9.3 0.0 all-gather.6.cloned.1.call-start
  9.4 0.9 convert_element_type.100
  10.3 0.9 convert_bitcast_fusion
  11.2 0.7 pad_maximum_fusion
  11.9 0.0 all-gather.6.cloned.1.call-update
  11.9 1.1 copy.30
  13.0 1.3 broadcast_in_dim.9
  14.3 10.5 %all-to-all-start = ((bf16[8,384,256]{1,2,0:T(8,128)(2,1)}), bf16[8,384,256]{1,2,0:T(8,128)(2,1)S(1)}, u32[]{:S(2)}, u32[]{:S(2)}) async-start(bf16[8,384,256]{1,2,0:T(8,128)(2,1)} %broadcast_in_dim.9), calls=%async_computation | async-start | bytes 3145728 | tf_op jit(solution)/shard_map/all_to_all | solution.py:28
  24.8 42.5 %all-gather = f32[64,32,2]{1,2,0:T(2,128)S(1)} all-gather(f32[1,32,2]{1,2,0:T(2,128)S(1)} %maximum_bitcast_fusion), channel_id=1, replica_groups=mesh['fs'=64,'tp'=8] {'fs'}, dimensions={0}, use_global_device_ids=true | all-gather | bytes 16640 | tf_op jit(solution)/shard_map/all_gather | solution.py:12
  67.3 0.1 reshape.91
  67.4 0.0 all-to-all-done
  67.4 0.4 multiply_reduce_fusion.1
  67.8 0.0 copy-done.2
  67.8 0.0 copy-start.9
  67.9 0.4 fusion.7
  68.3 0.0 copy-start.4
  68.3 0.0 copy-start.1
  68.3 0.0 copy-start.5
  68.3 0.0 copy-start.10
  68.3 25.8 %all-gather.4.cloned.1.call-done = bf16[2048,384]{1,0:T(8,128)(2,1)} async-done(((bf16[32,384]{1,0:T(8,128)(2,1)}), bf16[2048,384]{1,0:T(8,128)(2,1)}) %all-gather.4.cloned.1.call-update) | async-done | bytes 1572880 | tf_op jit(solution)/shard_map/all_gather | solution.py:12
  94.1 1.8 multiply_reduce_fusion.2
  95.8 0.6 broadcast_in_dim.10
  96.5 9.5 %all-to-all-start.1 = ((f32[8,1,384]{2,1,0:T(1,128)}), f32[8,1,384]{2,1,0:T(1,128)S(1)}, u32[]{:S(2)}, u32[]{:S(2)}) async-start(f32[8,1,384]{2,1,0:T(1,128)} %broadcast_in_dim.10), calls=%async_computation.1 | async-start | bytes 24576 | tf_op jit(solution)/shard_map/all_to_all | solution.py:28
  106.0 4.6 %all-to-all-done.1 = f32[8,1,384]{2,1,0:T(1,128)S(1)} async-done(((f32[8,1,384]{2,1,0:T(1,128)}), f32[8,1,384]{2,1,0:T(1,128)S(1)}, u32[]{:S(2)}, u32[]{:S(2)}) %all-to-all-start.1) | async-done | bytes 12320 | tf_op jit(solution)/shard_map/all_to_all | solution.py:28
  110.7 0.1 multiply_convert_fusion.3
  110.8 0.2 fusion.14
  111.0 3.0 %multiply_convert_fusion.1 = bf16[384,2048]{1,0:T(8,128)(2,1)S(1)} fusion(f32[2048]{0:T(1024)S(1)} %bitcast.66, bf16[2048,384]{1,0:T(8,128)(2,1)} %all-gather.4.cloned.1.call-done, f32[384,128]{1,0:T(8,128)S(1)} %bitcast.64, bf16[384,2048]{0,1:T(8,128)(2,1)S(1)} %fusion.7, f32[128]{0:T(128)S(1)} %copy-done.10), kind=kOutput, calls=%fused_computation.14 | convolution fusion | flops 404766720 | bytes 4399616 | tf_op jit(solution)/shard_map/dot_general | solution.py:108
  114.0 0.1 copy.42
  114.2 23.7 %all_to_all.26 = bf16[8,384,256]{2,1,0:T(8,128)(2,1)S(1)} all-to-all(bf16[8,384,256]{2,1,0:T(8,128)(2,1)S(1)} %bitcast.59), channel_id=1, replica_groups=mesh['fs'=64,'tp'=8] {'tp'}, dimensions={0} | all-to-all | bytes 3145728 | tf_op jit(solution)/shard_map/all_to_all | solution.py:48
  137.8 0.2 convert_reduce_fusion.1
  138.1 0.7 copy-done
  138.8 0.2 copy.34
  139.0 0.1 broadcast_in_dim.12
  139.1 24.1 %all_to_all.27 = bf16[8,384,256]{1,2,0:T(8,128)(2,1)S(1)} all-to-all(bf16[8,384,256]{1,2,0:T(8,128)(2,1)S(1)} %broadcast_in_dim.12), channel_id=1, replica_groups=mesh['fs'=64,'tp'=8] {'tp'}, dimensions={0} | all-to-all | bytes 3145728 | tf_op jit(solution)/shard_map/all_to_all | solution.py:28
  163.2 0.4 multiply_reduce_fusion
  163.6 0.3 copy-done.3
  163.9 0.4 fusion.5
  164.3 33.2 %all-gather.6.cloned.1.call-done = bf16[2048,2048]{1,0:T(8,128)(2,1)} async-done(((bf16[32,2048]{1,0:T(8,128)(2,1)}), bf16[2048,2048]{1,0:T(8,128)(2,1)}) %all-gather.6.cloned.1.call-update) | async-done | bytes 8388624 | tf_op jit(solution)/shard_map/all_gather | solution.py:12
  197.6 6.9 %multiply_convert_fusion = bf16[384,2048]{1,0:T(8,128)(2,1)S(1)} fusion(bf16[2048,2048]{1,0:T(8,128)(2,1)} %all-gather.6.cloned.1.call-done, f32[2048]{0:T(1024)S(1)} %bitcast.65, bf16[384,2048]{0,1:T(8,128)(2,1)S(1)} %fusion.5, f32[1024]{0:T(1024)S(1)} %copy-done.8), kind=kOutput, calls=%fused_computation.11 | convolution fusion | flops 3224371200 | bytes 11546624 | tf_op jit(solution)/shard_map/dot_general | solution.py:116
  204.5 0.1 copy.41
  204.6 25.5 %all_to_all.28 = bf16[8,384,256]{2,1,0:T(8,128)(2,1)S(1)} all-to-all(bf16[8,384,256]{2,1,0:T(8,128)(2,1)S(1)} %bitcast.60), channel_id=1, replica_groups=mesh['fs'=64,'tp'=8] {'tp'}, dimensions={0} | all-to-all | bytes 3145728 | tf_op jit(solution)/shard_map/all_to_all | solution.py:48
  230.2 0.2 convert_reduce_fusion
  230.4 0.7 add_convert_fusion
  (23 shorter events, 0.2 us)
Async XLA Ops:
  6.5 87.6 %all-gather.4.cloned.1.call-start = ((), (), s32[]{:S(2)}) async-start(), calls=%async_computation.5 | async-start | bytes 1597440 | tf_op jit(solution)/shard_map/all_gather | solution.py:12
  9.3 188.2 %all-gather.6.cloned.1.call-start = ((), (), s32[]{:S(2)}) async-start(), calls=%async_computation.6 | async-start | bytes 8519680 | tf_op jit(solution)/shard_map/all_gather | solution.py:12
  14.3 10.5 %copy-start.6 = (f32[32]{0:T(128)S(1)}, f32[32]{0:T(128)}, u32[]{:S(2)}) copy-start(f32[32]{0:T(128)} %param.31) | copy-start | bytes 388
  14.3 10.5 %copy-start.7 = (f32[32]{0:T(128)S(1)}, f32[32]{0:T(128)}, u32[]{:S(2)}) copy-start(f32[32]{0:T(128)} %param.26) | copy-start | bytes 388
  14.3 53.1 %all-to-all-start = ((bf16[8,384,256]{1,2,0:T(8,128)(2,1)}), bf16[8,384,256]{1,2,0:T(8,128)(2,1)S(1)}, u32[]{:S(2)}, u32[]{:S(2)}) async-start(bf16[8,384,256]{1,2,0:T(8,128)(2,1)} %broadcast_in_dim.9), calls=%async_computation | async-start | bytes 3145728 | tf_op jit(solution)/shard_map/all_to_all | solution.py:28
  24.7 43.1 %copy-start.2 = (f32[2048]{0:T(1024)S(1)}, f32[2048]{0:T(1024)}, u32[]{:S(2)}) copy-start(f32[2048]{0:T(1024)} %param.17) | copy-start | bytes 24580
  67.8 26.2 %copy-start.9 = (f32[128]{0:T(128)S(1)}, f32[128]{0:T(128)}, u32[]{:S(2)}) copy-start(f32[128]{0:T(128)} %param.21) | copy-start | bytes 1540
  68.3 42.4 %copy-start.4 = (f32[128]{0:T(128)S(1)}, f32[128]{0:T(128)}, u32[]{:S(2)}) copy-start(f32[128]{0:T(128)} %param.22) | copy-start | bytes 1540
  68.3 42.5 %copy-start.1 = (bf16[1,128,128]{2,1,0:T(8,128)(2,1)S(1)}, bf16[1,128,128]{2,1,0:T(8,128)(2,1)}, u32[]{:S(2)}) copy-start(bf16[1,128,128]{2,1,0:T(8,128)(2,1)} %param.23) | copy-start | bytes 98308
  68.3 42.5 %copy-start.5 = (f32[1,128]{1,0:T(1,128)S(1)}, f32[1,128]{1,0:T(1,128)}, u32[]{:S(2)}) copy-start(f32[1,128]{1,0:T(1,128)} %param.24) | copy-start | bytes 1540
  68.3 42.7 %copy-start.10 = (f32[128]{0:T(128)S(1)}, f32[128]{0:T(128)}, u32[]{:S(2)}) copy-start(f32[128]{0:T(128)} %param.20) | copy-start | bytes 1540
  96.5 14.2 %all-to-all-start.1 = ((f32[8,1,384]{2,1,0:T(1,128)}), f32[8,1,384]{2,1,0:T(1,128)S(1)}, u32[]{:S(2)}, u32[]{:S(2)}) async-start(f32[8,1,384]{2,1,0:T(1,128)} %broadcast_in_dim.10), calls=%async_computation.1 | async-start | bytes 24576 | tf_op jit(solution)/shard_map/all_to_all | solution.py:28
  137.8 0.9 copy-start
  163.2 0.7 copy-start.3
  163.9 33.7 %copy-start.8 = (f32[1024]{0:T(1024)S(1)}, f32[1024]{0:T(1024)}, u32[]{:S(2)}) copy-start(f32[1024]{0:T(1024)} %param.29) | copy-start | bytes 12292
Sparse Core Ops, SparseCore 0:
  10.3 83.7 all-gather.3
  97.1 100.3 all-gather.5
where the time goes:
time: 239 us; the launch traced here: 238 us
  blocking collectives  116 us (49%)
  waiting for transfers between devices  63.6 us (27%)
  starting transfers between devices  20 us (8%)
  between operations  13.6 us (6%)
  matrix products  11.9 us (5%)
  other arithmetic  8.33 us (3%)
  local copies, waits for them, and re-layouts  4.63 us (2%)
    all_gather x2, waiting for transfers between devices, gather_turned(): lax.all_gather(both, axis, axis=0, tiled=True)  59 us
    all_to_all x2, blocking collectives, summed_on_arrival(): blocks = lax.all_to_all(in_blocks(shard, dim, size), axis, 0, 0, tiled=True)  49.2 us
    all_gather x1, blocking collectives, gather_turned(): lax.all_gather(both, axis, axis=0, tiled=True)  42.5 us
    all_to_all x1, blocking collectives, sent_to_all(): lax.all_to_all(jnp.broadcast_to(shard[None], (size, *shard.shape)), axis,...  24.1 us
    all_to_all x2, starting transfers between devices, sent_to_all(): lax.all_to_all(jnp.broadcast_to(shard[None], (size, *shard.shape)), axis,...  20 us
    dot_general x1, matrix products, shards(): jnp.dot(hidden, down_cols, preferred_element_type=jnp.float32) * down_full  6.94 us
  transfers between devices with their start and end apart: 4, of which 3 were waited for; matrix products, arithmetic and copies ran while one was open for 5% of the time, Pallas kernels for 0%

commit v1 on v0

--- a/solution.py
+++ b/solution.py
@@ -6,10 +6,15 @@
 EPSILON = 1e-06
 
 
+def swapped_in(shard, axis, dim):
+    sent = jnp.stack([shard] * lax.axis_size(axis))
+    return jnp.concatenate(lax.all_to_all(sent, axis, 0, 0), axis=dim)
+
+
 def gather_turned(arrays, axis, dims):
     turned = [jnp.moveaxis(a, dim, 0) for a, dim in zip(arrays, dims)]
     both = jnp.concatenate([t.reshape(len(t), -1) for t in turned], axis=1)
-    result, at, finished = (lax.all_gather(both, axis, axis=0, tiled=True), 0, [])
+    result, at, finished = (swapped_in(both, axis, 0), 0, [])
     for t, dim in zip(turned, dims):
         section = result[:, at : at + t[0].size].reshape(-1, *t.shape[1:])
         finished.append(jnp.moveaxis(section, 0, dim))

time: 239 us -> 503 us (2.10)
  the two profiles are of different devices: /device:TPU:1 before, /device:TPU:40 now
where the time goes in v1:
time: 503 us
  waiting for transfers between devices  356 us (71%)
  blocking collectives  69.7 us (14%)
  starting transfers between devices  47.1 us (9%)
  matrix products  12.5 us (2%)
  local copies, waits for them, and re-layouts  12.2 us (2%)
    all_to_all x3, waiting for transfers between devices, swapped_in(): return jnp.concatenate(lax.all_to_all(sent, axis, 0, 0), axis=dim)  308 us
    all_to_all x2, blocking collectives, summed_on_arrival(): blocks = lax.all_to_all(in_blocks(shard, dim, size), axis, 0, 0, tiled=True)  69.7 us
    all_to_all x3, waiting for transfers between devices, sent_to_all(): lax.all_to_all(jnp.broadcast_to(shard[None], (size, *shard.shape)), axis,...  48.1 us
    all_to_all x3, starting transfers between devices, swapped_in(): return jnp.concatenate(lax.all_to_all(sent, axis, 0, 0), axis=dim)  35.6 us
    all_to_all x3, starting transfers between devices, sent_to_all(): lax.all_to_all(jnp.broadcast_to(shard[None], (size, *shard.shape)), axis,...  11.5 us
  transfers between devices with their start and end apart: 6, of which 6 were waited for; matrix products, arithmetic and copies ran while one was open for 1% of the time, Pallas kernels for 0%

profile of v1, /device:TPU:40, one launch (start us, length us, event | category | flops | bytes accessed | tf_op | source)
XLA Modules:
  0.0 502.6 jit_solution(14537414184500478883)
XLA Ops:
  0.0 0.7 pad_maximum_fusion.2
  0.7 0.6 stack.7
  1.3 16.1 %all-to-all-start.3 = ((f32[64,32,2]{1,2,0:T(2,128)}), f32[64,32,2]{1,2,0:T(2,128)S(1)}, u32[]{:S(2)}, u32[]{:S(2)}) async-start(f32[64,32,2]{1,2,0:T(2,128)} %stack.7), calls=%async_computation.3 | async-start | bytes 131072 | tf_op jit(solution)/shard_map/all_to_all | solution.py:11
  17.5 1.1 copy.32
  18.6 6.9 %all-to-all-done.3 = f32[64,32,2]{1,2,0:T(2,128)S(1)} async-done(((f32[64,32,2]{1,2,0:T(2,128)}), f32[64,32,2]{1,2,0:T(2,128)S(1)}, u32[]{:S(2)}, u32[]{:S(2)}) %all-to-all-start.3) | async-done | bytes 16416 | tf_op jit(solution)/shard_map/all_to_all | solution.py:11
  25.4 1.3 broadcast_in_dim.9
  26.7 4.4 all-to-all-start
  31.2 0.0 copy-done.4
  31.2 0.0 copy-done.5
  31.2 0.0 copy-done.6
  31.2 21.5 %all-to-all-done = bf16[8,384,256]{1,2,0:T(8,128)(2,1)S(1)} async-done(((bf16[8,384,256]{1,2,0:T(8,128)(2,1)}), bf16[8,384,256]{1,2,0:T(8,128)(2,1)S(1)}, u32[]{:S(2)}, u32[]{:S(2)}) %all-to-all-start) | async-done | bytes 1572896 | tf_op jit(solution)/shard_map/all_to_all | solution.py:33
  52.7 1.3 stack.6
  54.0 8.8 %all-to-all-start.1 = ((bf16[64,32,384]{2,1,0:T(8,128)(2,1)}), bf16[64,32,384]{2,1,0:T(8,128)(2,1)S(1)}, u32[]{:S(2)}, u32[]{:S(2)}) async-start(bf16[64,32,384]{2,1,0:T(8,128)(2,1)} %stack.6), calls=%async_computation.1 | async-start | bytes 3145728 | tf_op jit(solution)/shard_map/all_to_all | solution.py:11
  62.9 0.0 copy-start.7
  62.9 0.1 reshape.102
  63.0 0.4 multiply_reduce_fusion.1
  63.4 0.2 copy-done.7
  63.6 1.6 fusion.7
  65.1 36.3 %all-to-all-done.1 = bf16[64,32,384]{2,1,0:T(8,128)(2,1)S(1)} async-done(((bf16[64,32,384]{2,1,0:T(8,128)(2,1)}), bf16[64,32,384]{2,1,0:T(8,128)(2,1)S(1)}, u32[]{:S(2)}, u32[]{:S(2)}) %all-to-all-start.1) | async-done | bytes 1572896 | tf_op jit(solution)/shard_map/all_to_all | solution.py:11
  101.4 0.0 copy-start.13
  101.4 2.1 multiply_reduce_fusion.2
  103.6 0.6 broadcast_in_dim.10
  104.2 3.3 all-to-all-start.2
  107.6 5.2 %all-to-all-done.2 = f32[8,1,384]{2,1,0:T(1,128)S(1)} async-done(((f32[8,1,384]{2,1,0:T(1,128)}), f32[8,1,384]{2,1,0:T(1,128)S(1)}, u32[]{:S(2)}, u32[]{:S(2)}) %all-to-all-start.2) | async-done | bytes 12320 | tf_op jit(solution)/shard_map/all_to_all | solution.py:33
  112.9 0.1 multiply_convert_fusion.3
  113.0 0.2 fusion.14
  113.2 3.2 multiply_convert_fusion.1
  116.4 0.1 copy.44
  116.5 24.0 %all_to_all.41 = bf16[8,384,256]{2,1,0:T(8,128)(2,1)S(1)} all-to-all(bf16[8,384,256]{2,1,0:T(8,128)(2,1)S(1)} %bitcast.59), channel_id=1, replica_groups=mesh['fs'=64,'tp'=8] {'tp'}, dimensions={0} | all-to-all | bytes 3145728 | tf_op jit(solution)/shard_map/all_to_all | solution.py:53
  140.6 0.2 convert_reduce_fusion.1
  140.8 0.7 copy-done
  141.5 0.2 copy.36
  141.7 1.3 broadcast_in_dim.12
  143.0 3.7 all-to-all-start.5
  146.8 0.0 copy-done.2
  146.8 21.4 %all-to-all-done.5 = bf16[8,384,256]{1,2,0:T(8,128)(2,1)S(1)} async-done(((bf16[8,384,256]{1,2,0:T(8,128)(2,1)}), bf16[8,384,256]{1,2,0:T(8,128)(2,1)S(1)}, u32[]{:S(2)}, u32[]{:S(2)}) %all-to-all-start.5) | async-done | bytes 1572896 | tf_op jit(solution)/shard_map/all_to_all | solution.py:33
  168.2 4.3 stack.8
  172.5 10.6 %all-to-all-start.6 = ((bf16[64,32,2048]{2,1,0:T(8,128)(2,1)}), bf16[64,32,2048]{2,1,0:T(8,128)(2,1)}, u32[]{:S(2)}, u32[]{:S(2)}) async-start(bf16[64,32,2048]{2,1,0:T(8,128)(2,1)} %stack.8), calls=%async_computation.6 | async-start | bytes 16777216 | tf_op jit(solution)/shard_map/all_to_all | solution.py:11
  183.1 0.0 copy-start.8
  183.1 0.4 multiply_reduce_fusion
  183.6 0.3 copy-done.8
  183.8 0.4 fusion.5
  184.2 264.7 %all-to-all-done.6 = bf16[64,32,2048]{2,1,0:T(8,128)(2,1)} async-done(((bf16[64,32,2048]{2,1,0:T(8,128)(2,1)}), bf16[64,32,2048]{2,1,0:T(8,128)(2,1)}, u32[]{:S(2)}, u32[]{:S(2)}) %all-to-all-start.6) | async-done | bytes 8388640 | tf_op jit(solution)/shard_map/all_to_all | solution.py:11
  449.0 6.9 %multiply_convert_fusion = bf16[384,2048]{1,0:T(8,128)(2,1)S(1)} fusion(bf16[2048,2048]{1,0:T(8,128)(2,1)} %bitcast.18, f32[2048]{0:T(1024)S(1)} %bitcast.67, bf16[384,2048]{0,1:T(8,128)(2,1)S(1)} %fusion.5, f32[1024]{0:T(1024)S(1)} %copy-done.11), kind=kOutput, calls=%fused_computation.11 | convolution fusion | flops 3224371200 | bytes 11546624 | tf_op jit(solution)/shard_map/dot_general | solution.py:121
  455.9 0.1 copy.43
  456.0 45.6 %all_to_all.42 = bf16[8,384,256]{2,1,0:T(8,128)(2,1)S(1)} all-to-all(bf16[8,384,256]{2,1,0:T(8,128)(2,1)S(1)} %bitcast.60), channel_id=1, replica_groups=mesh['fs'=64,'tp'=8] {'tp'}, dimensions={0} | all-to-all | bytes 3145728 | tf_op jit(solution)/shard_map/all_to_all | solution.py:53
  501.6 0.2 convert_reduce_fusion
  501.9 0.7 add_convert_fusion
  (32 shorter events, 0.2 us)
Async XLA Ops:
  1.3 24.1 %all-to-all-start.3 = ((f32[64,32,2]{1,2,0:T(2,128)}), f32[64,32,2]{1,2,0:T(2,128)S(1)}, u32[]{:S(2)}, u32[]{:S(2)}) async-start(f32[64,32,2]{1,2,0:T(2,128)} %stack.7), calls=%async_computation.3 | async-start | bytes 131072 | tf_op jit(solution)/shard_map/all_to_all | solution.py:11
  26.7 4.4 copy-start.4
  26.7 4.5 copy-start.5
  26.7 4.5 copy-start.6
  26.7 26.0 %all-to-all-start = ((bf16[8,384,256]{1,2,0:T(8,128)(2,1)}), bf16[8,384,256]{1,2,0:T(8,128)(2,1)S(1)}, u32[]{:S(2)}, u32[]{:S(2)}) async-start(bf16[8,384,256]{1,2,0:T(8,128)(2,1)} %broadcast_in_dim.9), calls=%async_computation | async-start | bytes 3145728 | tf_op jit(solution)/shard_map/all_to_all | solution.py:33
  54.0 47.4 %all-to-all-start.1 = ((bf16[64,32,384]{2,1,0:T(8,128)(2,1)}), bf16[64,32,384]{2,1,0:T(8,128)(2,1)S(1)}, u32[]{:S(2)}, u32[]{:S(2)}) async-start(bf16[64,32,384]{2,1,0:T(8,128)(2,1)} %stack.6), calls=%async_computation.1 | async-start | bytes 3145728 | tf_op jit(solution)/shard_map/all_to_all | solution.py:11
  62.9 0.7 copy-start.7
  63.6 37.9 %copy-start.12 = (f32[128]{0:T(128)S(1)}, f32[128]{0:T(128)}, u32[]{:S(2)}) copy-start(f32[128]{0:T(128)} %param.21) | copy-start | bytes 1540
  101.4 11.4 %copy-start.9 = (f32[128]{0:T(128)S(1)}, f32[128]{0:T(128)}, u32[]{:S(2)}) copy-start(f32[128]{0:T(128)} %param.22) | copy-start | bytes 1540
  101.4 11.6 %copy-start.3 = (bf16[1,128,128]{2,1,0:T(8,128)(2,1)S(1)}, bf16[1,128,128]{2,1,0:T(8,128)(2,1)}, u32[]{:S(2)}) copy-start(bf16[1,128,128]{2,1,0:T(8,128)(2,1)} %param.23) | copy-start | bytes 98308
  101.4 11.6 %copy-start.10 = (f32[1,128]{1,0:T(1,128)S(1)}, f32[1,128]{1,0:T(1,128)}, u32[]{:S(2)}) copy-start(f32[1,128]{1,0:T(1,128)} %param.24) | copy-start | bytes 1540
  101.4 11.7 %copy-start.13 = (f32[128]{0:T(128)S(1)}, f32[128]{0:T(128)}, u32[]{:S(2)}) copy-start(f32[128]{0:T(128)} %param.20) | copy-start | bytes 1540
  104.2 8.6 %all-to-all-start.2 = ((f32[8,1,384]{2,1,0:T(1,128)}), f32[8,1,384]{2,1,0:T(1,128)S(1)}, u32[]{:S(2)}, u32[]{:S(2)}) async-start(f32[8,1,384]{2,1,0:T(1,128)} %broadcast_in_dim.10), calls=%async_computation.2 | async-start | bytes 24576 | tf_op jit(solution)/shard_map/all_to_all | solution.py:33
  140.6 0.9 copy-start
  143.0 3.7 copy-start.1
  143.0 3.8 copy-start.2
  143.0 25.2 %all-to-all-start.5 = ((bf16[8,384,256]{1,2,0:T(8,128)(2,1)}), bf16[8,384,256]{1,2,0:T(8,128)(2,1)S(1)}, u32[]{:S(2)}, u32[]{:S(2)}) async-start(bf16[8,384,256]{1,2,0:T(8,128)(2,1)} %broadcast_in_dim.12), calls=%async_computation.5 | async-start | bytes 3145728 | tf_op jit(solution)/shard_map/all_to_all | solution.py:33
  172.5 276.5 %all-to-all-start.6 = ((bf16[64,32,2048]{2,1,0:T(8,128)(2,1)}), bf16[64,32,2048]{2,1,0:T(8,128)(2,1)}, u32[]{:S(2)}, u32[]{:S(2)}) async-start(bf16[64,32,2048]{2,1,0:T(8,128)(2,1)} %stack.8), calls=%async_computation.6 | async-start | bytes 16777216 | tf_op jit(solution)/shard_map/all_to_all | solution.py:11
  183.1 0.7 copy-start.8
  183.8 265.2 %copy-start.11 = (f32[1024]{0:T(1024)S(1)}, f32[1024]{0:T(1024)}, u32[]{:S(2)}) copy-start(f32[1024]{0:T(1024)} %param.29) | copy-start | bytes 12292
